TPU v7x, 512 devices: a whole 4x4x16 slice. The times are simulated.
512 devices in a mesh: fs: 16 (over y, x), tp: 32 (over z, core).
Axes of the slice: x: 4, y: 4, z: 16, core: 2. Of those that a mesh axis runs over, the one named last changes fastest.
Arguments:
- x_later: bfloat16 [6144, 2048], P('fs'), may hold values from -6 to 6
- x_earlier: bfloat16 [6144, 2048], P('fs'), may hold values from -6 to 6
- cot_hidden: bfloat16 [6144, 4096], P('fs', 'tp'), may hold values from -6 to 6
- w_gate: bfloat16 [2048, 4096], P('fs', 'tp'), may hold values from -0.125 to 0.125
- w_up: bfloat16 [2048, 4096], P('fs', 'tp'), may hold values from -0.125 to 0.125
- grad_gate: float32 [2048, 4096], P('fs', 'tp'), may hold values from -192 to 192
- grad_up: float32 [2048, 4096], P('fs', 'tp'), may hold values from -192 to 192
Outputs:
- hidden_later: bfloat16 [6144, 4096], P('fs', 'tp')
- grad_input: bfloat16 [6144, 2048], P('fs')
- new_grad_gate: float32 [2048, 4096], P('fs', 'tp')
- new_grad_up: float32 [2048, 4096], P('fs', 'tp')
All inputs are finite; a program needn't handle non-finite values.
Results may differ from a plain program's by a relative error of at most 0.018.
Values may be sent and summed in bfloat16 or wider, within the bound.
A program may use at most 64 MiB of HBM per device.

v0:
```python
import jax
import jax.numpy as jnp
from jax import lax
from jax.sharding import PartitionSpec as P


def contract_last(left, right):
    return lax.dot_general(
        left, right, (((1,), (1,)), ((), ())), preferred_element_type=jnp.float32
    )


def contract_first(left, right):
    return lax.dot_general(
        left, right, (((0,), (0,)), ((), ())), preferred_element_type=jnp.float32
    )


def per_device(x_later, x_earlier, cot_hidden, w_gate, w_up, grad_gate, grad_up):
    hidden_width = w_gate.shape[1]
    whole_gate, whole_up = (
        lax.all_gather(w_gate, "fs", axis=0, tiled=True),
        lax.all_gather(w_up, "fs", axis=0, tiled=True),
    )
    gate_later = jnp.dot(x_later, whole_gate, preferred_element_type=jnp.float32)
    up_later = jnp.dot(x_later, whole_up, preferred_element_type=jnp.float32)
    gate_earlier = jnp.dot(x_earlier, whole_gate, preferred_element_type=jnp.float32)
    up_earlier = jnp.dot(x_earlier, whole_up, preferred_element_type=jnp.float32)
    hidden_later = (jax.nn.silu(gate_later) * up_later).astype(jnp.bfloat16)
    sigma = jax.nn.sigmoid(gate_earlier)
    cotangent = cot_hidden.astype(jnp.float32)
    delta_up = (cotangent * gate_earlier * sigma).astype(jnp.bfloat16)
    delta_gate = (cotangent * up_earlier * sigma * (1.0 + gate_earlier * (1.0 - sigma))).astype(
        jnp.bfloat16
    )
    grad_share = lax.psum_scatter(
        (contract_last(delta_gate, whole_gate) + contract_last(delta_up, whole_up)).astype(
            jnp.bfloat16
        ),
        "tp",
        scatter_dimension=0,
        tiled=True,
    )
    grad_input = lax.all_gather(grad_share, "tp", axis=0, tiled=True)
    deltas = jnp.concatenate([delta_gate, delta_up], 1)
    summed = lax.psum_scatter(
        contract_first(x_earlier, deltas).astype(jnp.bfloat16),
        "fs",
        scatter_dimension=0,
        tiled=True,
    ).astype(jnp.float32)
    new_grad_gate = grad_gate + summed[:, :hidden_width]
    new_grad_up = grad_up + summed[:, hidden_width:]
    return (hidden_later, grad_input, new_grad_gate, new_grad_up)


def solution(mesh):
    placed = (
        P("fs", None),
        P("fs", None),
        P("fs", "tp"),
        P("fs", "tp"),
        P("fs", "tp"),
        P("fs", "tp"),
        P("fs", "tp"),
    )
    return jax.shard_map(
        per_device,
        mesh=mesh,
        in_specs=placed,
        out_specs=(P("fs", "tp"), P("fs", None), P("fs", "tp"), P("fs", "tp")),
        check_vma=False,
    )
```

profile of v0, /device:TPU:1, one launch (start us, length us, event | category | flops | bytes accessed | tf_op | source)
XLA Modules:
  0.0 242.5 jit_solution(5092972627354294884)
XLA Ops:
  8.0 0.0 copy-start
  8.0 0.0 reduce-scatter.6.cloned.1.call-start
  8.1 20.1 %all_gather.10 = bf16[2048,128]{1,0:T(8,128)(2,1)S(1)} all-gather(bf16[128,128]{1,0:T(8,128)(2,1)} %param.11), channel_id=1, replica_groups=mesh['fs'=16,'tp'=32] {'fs'}, dimensions={0}, use_global_device_ids=true | all-gather | bytes 557056 | tf_op jit(solution)/shard_map/all_gather | solution.py:23
  28.1 0.0 copy-start.3
  28.1 17.9 %all_gather.9 = bf16[2048,128]{1,0:T(8,128)(2,1)S(1)} all-gather(bf16[128,128]{1,0:T(8,128)(2,1)} %param.10), channel_id=1, replica_groups=mesh['fs'=16,'tp'=32] {'fs'}, dimensions={0}, use_global_device_ids=true | all-gather | bytes 557056 | tf_op jit(solution)/shard_map/all_gather | solution.py:22
  46.1 0.0 copy-done
  46.1 0.0 copy-start.1
  46.1 0.0 copy-start.9
  46.1 1.7 fusion.7
  47.8 0.0 copy-done.3
  47.8 0.0 copy-done.9
  47.8 0.6 fusion.5
  48.4 0.7 fusion.1
  49.1 1.3 copy.37
  50.4 0.0 reduce-scatter.6.cloned.1.call-update
  50.4 0.0 all-gather.3.cloned.1.call-start
  50.5 0.0 copy-done.1
  50.5 0.0 copy-start.4
  50.5 0.6 fusion.13
  51.1 0.5 copy-done.4
  51.5 0.6 add_convert_fusion
  52.1 0.0 copy-start.7
  52.1 0.0 copy-start.8
  52.2 74.8 %fusion = bf16[16,2048]{1,0:T(8,128)(2,1)S(1)} fusion(bf16[384,2048]{1,0:T(8,128)(2,1)S(1)} %add_convert_fusion), kind=kCustom, calls=%all-reduce-scatter | all-reduce-scatter fusion | flops 1048577 | bytes 1640448
  127.0 0.0 copy-start.2
  127.0 3.4 %collective-permute-start.6 = (bf16[16,2048]{1,0:T(8,128)(2,1)S(1)}, bf16[16,2048]{1,0:T(8,128)(2,1)S(1)}, u32[]{:S(2)}, u32[]{:S(2)}) collective-permute-start(bf16[16,2048]{1,0:T(8,128)(2,1)S(1)} %fusion), channel_id=1, source_target_pairs={{0,7},{1,8},{2,9},{3,10},{4,11},{5,12},{6,13},{7,14},{8,15},{9,16}... | collective-permute-start | bytes 196616
  130.4 4.5 %collective-permute-start.5 = (bf16[16,2048]{1,0:T(8,128)(2,1)S(1)}, bf16[16,2048]{1,0:T(8,128)(2,1)S(1)}, u32[]{:S(2)}, u32[]{:S(2)}) collective-permute-start(bf16[16,2048]{1,0:T(8,128)(2,1)S(1)} %fusion), channel_id=1, source_target_pairs={{0,6},{1,7},{2,8},{3,9},{4,10},{5,11},{6,12},{7,13},{8,14},{9,15},... | collective-permute-start | bytes 196616
  134.9 6.2 %collective-permute-start.7 = (bf16[12,2048]{1,0:T(8,128)(2,1)S(1)}, bf16[12,2048]{1,0:T(8,128)(2,1)S(1)}, u32[]{:S(2)}, u32[]{:S(2)}) collective-permute-start(bf16[12,2048]{1,0:T(8,128)(2,1)S(1)} %slice.10), channel_id=1, source_target_pairs={{0,8},{1,9},{2,10},{3,11},{4,12},{5,13},{6,14},{7,15},{8,16},{9,17... | collective-permute-start | bytes 147464
  141.1 1.7 collective-permute-start.4
  142.8 6.4 %collective-permute-start.3 = (bf16[16,2048]{1,0:T(8,128)(2,1)S(1)}, bf16[16,2048]{1,0:T(8,128)(2,1)S(1)}, u32[]{:S(2)}, u32[]{:S(2)}) collective-permute-start(bf16[16,2048]{1,0:T(8,128)(2,1)S(1)} %fusion), channel_id=1, source_target_pairs={{0,4},{1,5},{2,6},{3,7},{4,8},{5,9},{6,10},{7,11},{8,12},{9,13},{1... | collective-permute-start | bytes 196616
  149.3 0.0 collective-permute-done.7
  149.3 1.6 collective-permute-start.2
  150.9 0.0 collective-permute-done.6
  150.9 2.8 %collective-permute-start.1 = (bf16[16,2048]{1,0:T(8,128)(2,1)S(1)}, bf16[16,2048]{1,0:T(8,128)(2,1)S(1)}, u32[]{:S(2)}, u32[]{:S(2)}) collective-permute-start(bf16[16,2048]{1,0:T(8,128)(2,1)S(1)} %fusion), channel_id=1, source_target_pairs={{0,2},{1,3},{2,4},{3,5},{4,6},{5,7},{6,8},{7,9},{8,10},{9,11},{10,... | collective-permute-start | bytes 196616
  153.7 0.0 collective-permute-done.5
  153.7 2.2 collective-permute-start
  155.9 1.3 dynamic-slice.4
  157.8 0.0 collective-permute-done.4
  157.8 0.0 collective-permute-done.3
  157.9 0.0 collective-permute-done.2
  157.9 0.0 collective-permute-done.1
  157.9 0.0 collective-permute-done
  157.9 1.5 concatenate.4
  159.4 0.0 copy-start.5
  159.4 0.7 dynamic-slice_bitcast_fusion
  160.0 0.0 all-gather.3.cloned.1.call-update
  160.1 0.0 copy-done.7
  160.1 0.1 copy.32
  160.2 0.0 copy-done.8
  160.2 0.1 copy.31
  160.3 0.0 copy-done.2
  160.3 0.0 copy-start.6
  160.3 2.1 fusion.12
  162.4 0.0 copy-done.5
  162.4 0.0 copy-done.6
  162.4 1.2 fusion.4
  163.6 0.0 reduce-scatter.6.cloned.1.call-done
  163.6 0.9 copy.38
  164.6 0.7 copy.33
  165.4 0.7 copy.34
  166.1 65.4 %all-gather.3.cloned.1.call-done = bf16[32,12,2048]{2,1,0:T(8,128)(2,1)} async-done(((bf16[1,12,2048]{2,1,0:T(8,128)(2,1)}), bf16[32,12,2048]{2,1,0:T(8,128)(2,1)}) %all-gather.3.cloned.1.call-update) | async-done | bytes 1572880 | tf_op jit(solution)/shard_map/all_gather | solution.py:44
  231.4 3.6 %reshape.9 = bf16[384,2048]{1,0:T(8,128)(2,1)} reshape(bf16[32,12,2048]{2,1,0:T(8,128)(2,1)} %all-gather.3.cloned.1.call-done) | data formatting | bytes 3145728
  (3 shorter events, 0.1 us)
Async XLA Ops:
  8.0 38.1 %copy-start = (bf16[384,2048]{1,0:T(8,128)(2,1)S(1)}, bf16[384,2048]{1,0:T(8,128)(2,1)}, u32[]{:S(2)}) copy-start(bf16[384,2048]{1,0:T(8,128)(2,1)} %param.8) | copy-start | bytes 4718596
  8.0 155.6 %reduce-scatter.6.cloned.1.call-start = ((), (), s32[]{:S(2)}) async-start(), calls=%async_computation.2 | async-start | bytes 1114112
  28.1 19.6 %copy-start.3 = (bf16[2048,128]{1,0:T(8,128)(2,1)}, bf16[2048,128]{1,0:T(8,128)(2,1)S(1)}, u32[]{:S(2)}) copy-start(bf16[2048,128]{1,0:T(8,128)(2,1)S(1)} %all_gather.10) | copy-start | bytes 1572868
  46.1 4.4 %copy-start.1 = (bf16[2048,128]{1,0:T(8,128)(2,1)}, bf16[2048,128]{1,0:T(8,128)(2,1)S(1)}, u32[]{:S(2)}) copy-start(bf16[2048,128]{1,0:T(8,128)(2,1)S(1)} %all_gather.9) | copy-start | bytes 1572868
  46.1 1.7 copy-start.9
  50.4 181.0 %all-gather.3.cloned.1.call-start = ((), (), s32[]{:S(2)}) async-start(), calls=%async_computation.1 | async-start | bytes 2162688 | tf_op jit(solution)/shard_map/all_gather | solution.py:44
  50.5 1.0 copy-start.4
  52.1 107.9 %copy-start.7 = (f32[128,128]{1,0:T(8,128)S(1)}, f32[128,128]{1,0:T(8,128)}, u32[]{:S(2)}) copy-start(f32[128,128]{1,0:T(8,128)} %param.13) | copy-start | bytes 196612
  52.1 108.0 %copy-start.8 = (f32[128,128]{1,0:T(8,128)S(1)}, f32[128,128]{1,0:T(8,128)}, u32[]{:S(2)}) copy-start(f32[128,128]{1,0:T(8,128)} %param.12) | copy-start | bytes 196612
  127.0 33.3 %copy-start.2 = (bf16[2048,128]{1,0:T(8,128)(2,1)S(1)}, bf16[2048,128]{1,0:T(8,128)(2,1)}, u32[]{:S(2)}) copy-start(bf16[2048,128]{1,0:T(8,128)(2,1)} %copy-done.1) | copy-start | bytes 1572868
  127.0 24.0 %collective-permute-start.6 = (bf16[16,2048]{1,0:T(8,128)(2,1)S(1)}, bf16[16,2048]{1,0:T(8,128)(2,1)S(1)}, u32[]{:S(2)}, u32[]{:S(2)}) collective-permute-start(bf16[16,2048]{1,0:T(8,128)(2,1)S(1)} %fusion), channel_id=1, source_target_pairs={{0,7},{1,8},{2,9},{3,10},{4,11},{5,12},{6,13},{7,14},{8,15},{9,16}... | collective-permute-start | bytes 196616
  130.4 23.3 %collective-permute-start.5 = (bf16[16,2048]{1,0:T(8,128)(2,1)S(1)}, bf16[16,2048]{1,0:T(8,128)(2,1)S(1)}, u32[]{:S(2)}, u32[]{:S(2)}) collective-permute-start(bf16[16,2048]{1,0:T(8,128)(2,1)S(1)} %fusion), channel_id=1, source_target_pairs={{0,6},{1,7},{2,8},{3,9},{4,10},{5,11},{6,12},{7,13},{8,14},{9,15},... | collective-permute-start | bytes 196616
  134.9 14.4 %collective-permute-start.7 = (bf16[12,2048]{1,0:T(8,128)(2,1)S(1)}, bf16[12,2048]{1,0:T(8,128)(2,1)S(1)}, u32[]{:S(2)}, u32[]{:S(2)}) collective-permute-start(bf16[12,2048]{1,0:T(8,128)(2,1)S(1)} %slice.10), channel_id=1, source_target_pairs={{0,8},{1,9},{2,10},{3,11},{4,12},{5,13},{6,14},{7,15},{8,16},{9,17... | collective-permute-start | bytes 147464
  141.1 16.7 %collective-permute-start.4 = (bf16[16,2048]{1,0:T(8,128)(2,1)S(1)}, bf16[16,2048]{1,0:T(8,128)(2,1)S(1)}, u32[]{:S(2)}, u32[]{:S(2)}) collective-permute-start(bf16[16,2048]{1,0:T(8,128)(2,1)S(1)} %fusion), channel_id=1, source_target_pairs={{0,5},{1,6},{2,7},{3,8},{4,9},{5,10},{6,11},{7,12},{8,13},{9,14},{... | collective-permute-start | bytes 196616
  142.8 15.0 %collective-permute-start.3 = (bf16[16,2048]{1,0:T(8,128)(2,1)S(1)}, bf16[16,2048]{1,0:T(8,128)(2,1)S(1)}, u32[]{:S(2)}, u32[]{:S(2)}) collective-permute-start(bf16[16,2048]{1,0:T(8,128)(2,1)S(1)} %fusion), channel_id=1, source_target_pairs={{0,4},{1,5},{2,6},{3,7},{4,8},{5,9},{6,10},{7,11},{8,12},{9,13},{1... | collective-permute-start | bytes 196616
  149.3 8.6 %collective-permute-start.2 = (bf16[16,2048]{1,0:T(8,128)(2,1)S(1)}, bf16[16,2048]{1,0:T(8,128)(2,1)S(1)}, u32[]{:S(2)}, u32[]{:S(2)}) collective-permute-start(bf16[16,2048]{1,0:T(8,128)(2,1)S(1)} %fusion), channel_id=1, source_target_pairs={{0,3},{1,4},{2,5},{3,6},{4,7},{5,8},{6,9},{7,10},{8,11},{9,12},{10... | collective-permute-start | bytes 196616
  150.9 6.9 %collective-permute-start.1 = (bf16[16,2048]{1,0:T(8,128)(2,1)S(1)}, bf16[16,2048]{1,0:T(8,128)(2,1)S(1)}, u32[]{:S(2)}, u32[]{:S(2)}) collective-permute-start(bf16[16,2048]{1,0:T(8,128)(2,1)S(1)} %fusion), channel_id=1, source_target_pairs={{0,2},{1,3},{2,4},{3,5},{4,6},{5,7},{6,8},{7,9},{8,10},{9,11},{10,... | collective-permute-start | bytes 196616
  153.7 4.2 %collective-permute-start = (bf16[16,2048]{1,0:T(8,128)(2,1)S(1)}, bf16[16,2048]{1,0:T(8,128)(2,1)S(1)}, u32[]{:S(2)}, u32[]{:S(2)}) collective-permute-start(bf16[16,2048]{1,0:T(8,128)(2,1)S(1)} %fusion), channel_id=1, source_target_pairs={{0,1},{1,2},{2,3},{3,4},{4,5},{5,6},{6,7},{7,8},{8,9},{9,10},{10,1... | collective-permute-start | bytes 196616
  159.4 3.0 %copy-start.5 = (bf16[2048,128]{1,0:T(8,128)(2,1)S(1)}, bf16[2048,128]{1,0:T(8,128)(2,1)}, u32[]{:S(2)}) copy-start(bf16[2048,128]{1,0:T(8,128)(2,1)} %copy-done.3) | copy-start | bytes 1572868
  160.3 2.1 copy-start.6
Sparse Core Ops, SparseCore 0:
  50.6 100.0 reduce-scatter.5
Sparse Core Ops, SparseCore 1:
  160.1 71.2 all-gather.2
where the time goes:
time: 243 us; the launch traced here: 242 us
  blocking collectives  113 us (47%)
  waiting for transfers between devices  65.4 us (27%)
  starting transfers between devices  28.9 us (12%)
  between operations  16.5 us (7%)
  local copies, waits for them, and re-layouts  11.4 us (5%)
  matrix products  7.43 us (3%)
    unnamed x1, blocking collectives  74.8 us
    all_gather x1, waiting for transfers between devices, per_device(): grad_input = lax.all_gather(grad_share, 'tp', axis=0, tiled=True)  65.4 us
    unnamed x9, starting transfers between devices  28.9 us
    all_gather x1, blocking collectives, per_device(): lax.all_gather(w_up, 'fs', axis=0, tiled=True)  20.1 us
    all_gather x1, blocking collectives, per_device(): lax.all_gather(w_gate, 'fs', axis=0, tiled=True)  17.9 us
    unnamed x31, local copies, waits for them, and re-layouts  11.4 us
  transfers between devices with their start and end apart: 10, of which 1 were waited for; matrix products, arithmetic and copies ran while one was open for 35% of the time, Pallas kernels for 0%

commit v1 on v0

--- a/solution.py
+++ b/solution.py
@@ -41,7 +41,9 @@
         scatter_dimension=0,
         tiled=True,
     )
-    grad_input = lax.all_gather(grad_share, "tp", axis=0, tiled=True)
+    grad_input = jnp.concatenate(
+        lax.all_to_all(jnp.stack([grad_share] * lax.axis_size("tp")), "tp", 0, 0), axis=0
+    )
     deltas = jnp.concatenate([delta_gate, delta_up], 1)
     summed = lax.psum_scatter(
         contract_first(x_earlier, deltas).astype(jnp.bfloat16),

time: 243 us -> 279 us (1.15)
  waiting for transfers between devices: 65.4 us -> 90.2 us
  starting transfers between devices: 28.9 us -> 42 us
    unnamed x11 -> x10, waiting for transfers between devices: 0.06 us -> 85.6 us
    all_gather x1 -> x0, waiting for transfers between devices: 65.4 us -> none  [per_device(): grad_input = lax.all_gather(grad_share, 'tp', axis=0, tiled=True)]
    all_to_all x0 -> x1, starting transfers between devices: none -> 12.2 us  [per_device(): lax.all_to_all(jnp.stack([grad_share] * lax.axis_size('tp')), 'tp', 0, 0)]
    unnamed x31 -> x28, local copies, waits for them, and re-layouts: 11.4 us -> 6.72 us
    all_to_all x0 -> x1, waiting for transfers between devices: none -> 4.59 us  [per_device(): lax.all_to_all(jnp.stack([grad_share] * lax.axis_size('tp')), 'tp', 0, 0)]
    reshape x0 -> x1, local copies, waits for them, and re-layouts: none -> 3.6 us  [per_device(): jnp.concatenate(lax.all_to_all(jnp.stack([grad_share] * lax.axis_size('tp...]
  transfers between devices with their start and end apart: 10 -> 10, of which waited for: 1 -> 2; matrix products, arithmetic and copies ran while one was open for 35% -> 3% of each run, Pallas kernels for 0% -> 0%
where the time goes in v1:
time: 279 us; the launch traced here: 278 us
  blocking collectives  112 us (40%)
  waiting for transfers between devices  90.2 us (32%)
  starting transfers between devices  42 us (15%)
  between operations  15 us (5%)
  local copies, waits for them, and re-layouts  11.9 us (4%)
  matrix products  7.44 us (3%)
    unnamed x10, waiting for transfers between devices  85.6 us
    unnamed x1, blocking collectives  73.7 us
    unnamed x9, starting transfers between devices  29.7 us
    all_gather x1, blocking collectives, per_device(): lax.all_gather(w_up, 'fs', axis=0, tiled=True)  20.1 us
    all_gather x1, blocking collectives, per_device(): lax.all_gather(w_gate, 'fs', axis=0, tiled=True)  17.9 us
    all_to_all x1, starting transfers between devices, per_device(): lax.all_to_all(jnp.stack([grad_share] * lax.axis_size('tp')), 'tp', 0, 0)  12.2 us
    unnamed x28, local copies, waits for them, and re-layouts  6.72 us
  transfers between devices with their start and end apart: 10, of which 2 were waited for; matrix products, arithmetic and copies ran while one was open for 3% of the time, Pallas kernels for 0%

profile of v1, /device:TPU:1, one launch (start us, length us, event | category | flops | bytes accessed | tf_op | source)
XLA Modules:
  0.0 278.3 jit_solution(3751109749429655214)
XLA Ops:
  7.2 0.0 copy-start
  7.2 20.1 %all_gather.7 = bf16[2048,128]{1,0:T(8,128)(2,1)S(1)} all-gather(bf16[128,128]{1,0:T(8,128)(2,1)} %param.11), channel_id=1, replica_groups=mesh['fs'=16,'tp'=32] {'fs'}, dimensions={0}, use_global_device_ids=true | all-gather | bytes 557056 | tf_op jit(solution)/shard_map/all_gather | solution.py:23
  27.3 0.0 copy-start.3
  27.3 17.9 %all_gather.6 = bf16[2048,128]{1,0:T(8,128)(2,1)S(1)} all-gather(bf16[128,128]{1,0:T(8,128)(2,1)} %param.10), channel_id=1, replica_groups=mesh['fs'=16,'tp'=32] {'fs'}, dimensions={0}, use_global_device_ids=true | all-gather | bytes 557056 | tf_op jit(solution)/shard_map/all_gather | solution.py:22
  45.2 0.0 copy-done
  45.2 0.0 copy-start.1
  45.2 0.0 copy-start.8
  45.2 1.7 fusion.7
  46.9 0.0 copy-done.8
  46.9 0.6 fusion.5
  47.5 0.0 copy-done.1
  47.5 0.6 fusion.13
  48.1 0.0 copy-done.3
  48.1 0.6 add_convert_fusion
  48.7 73.7 %fusion = bf16[16,2048]{1,0:T(8,128)(2,1)S(1)} fusion(bf16[384,2048]{1,0:T(8,128)(2,1)S(1)} %add_convert_fusion), kind=kCustom, calls=%all-reduce-scatter | all-reduce-scatter fusion | flops 1048577 | bytes 1640448
  122.4 3.6 %collective-permute-start.6 = (bf16[16,2048]{1,0:T(8,128)(2,1)S(1)}, bf16[16,2048]{1,0:T(8,128)(2,1)S(1)}, u32[]{:S(2)}, u32[]{:S(2)}) collective-permute-start(bf16[16,2048]{1,0:T(8,128)(2,1)S(1)} %fusion), channel_id=1, source_target_pairs={{0,7},{1,8},{2,9},{3,10},{4,11},{5,12},{6,13},{7,14},{8,15},{9,16}... | collective-permute-start | bytes 196616
  126.0 4.3 %collective-permute-start.5 = (bf16[16,2048]{1,0:T(8,128)(2,1)S(1)}, bf16[16,2048]{1,0:T(8,128)(2,1)S(1)}, u32[]{:S(2)}, u32[]{:S(2)}) collective-permute-start(bf16[16,2048]{1,0:T(8,128)(2,1)S(1)} %fusion), channel_id=1, source_target_pairs={{0,6},{1,7},{2,8},{3,9},{4,10},{5,11},{6,12},{7,13},{8,14},{9,15},... | collective-permute-start | bytes 196616
  130.3 6.6 %collective-permute-start.7 = (bf16[12,2048]{1,0:T(8,128)(2,1)S(1)}, bf16[12,2048]{1,0:T(8,128)(2,1)S(1)}, u32[]{:S(2)}, u32[]{:S(2)}) collective-permute-start(bf16[12,2048]{1,0:T(8,128)(2,1)S(1)} %slice.10), channel_id=1, source_target_pairs={{0,8},{1,9},{2,10},{3,11},{4,12},{5,13},{6,14},{7,15},{8,16},{9,17... | collective-permute-start | bytes 147464
  136.9 1.3 collective-permute-start.4
  138.2 7.4 %collective-permute-start.3 = (bf16[16,2048]{1,0:T(8,128)(2,1)S(1)}, bf16[16,2048]{1,0:T(8,128)(2,1)S(1)}, u32[]{:S(2)}, u32[]{:S(2)}) collective-permute-start(bf16[16,2048]{1,0:T(8,128)(2,1)S(1)} %fusion), channel_id=1, source_target_pairs={{0,4},{1,5},{2,6},{3,7},{4,8},{5,9},{6,10},{7,11},{8,12},{9,13},{1... | collective-permute-start | bytes 196616
  145.5 0.0 collective-permute-done.7
  145.5 1.6 collective-permute-start.2
  147.2 0.0 collective-permute-done.6
  147.2 2.8 collective-permute-start.1
  150.0 0.0 collective-permute-done.5
  150.0 2.2 collective-permute-start
  152.2 1.3 dynamic-slice.4
  154.1 0.0 collective-permute-done.4
  154.1 0.0 collective-permute-done.3
  154.1 0.0 collective-permute-done.2
  154.1 0.0 collective-permute-done.1
  154.1 0.0 collective-permute-done
  154.1 1.5 concatenate.4
  155.6 1.6 stack.2
  157.2 12.2 %all-to-all-start = ((bf16[32,12,2048]{2,1,0:T(8,128)(2,1)}), bf16[32,12,2048]{2,1,0:T(8,128)(2,1)}, u32[]{:S(2)}, u32[]{:S(2)}) async-start(bf16[32,12,2048]{2,1,0:T(8,128)(2,1)} %stack.2), calls=%async_computation | async-start | bytes 4194304 | tf_op jit(solution)/shard_map/all_to_all | solution.py:45
  169.5 0.0 reduce-scatter.6.cloned.1.call-start
  169.5 0.7 fusion.1
  170.2 0.0 copy-start.6
  170.3 0.0 copy-start.7
  170.3 0.0 copy-start.2
  170.3 1.3 copy.37
  171.6 0.0 copy-start.4
  171.6 0.0 reduce-scatter.6.cloned.1.call-update
  171.6 0.0 copy-done.6
  171.6 0.1 copy.32
  171.7 0.0 copy-done.7
  171.7 0.1 copy.31
  171.8 0.0 copy-done.2
  171.8 0.0 copy-start.5
  171.8 2.1 fusion.12
  173.9 0.0 copy-done.4
  174.0 0.0 copy-done.5
  174.0 1.2 fusion.4
  175.2 85.6 %reduce-scatter.6.cloned.1.call-done = bf16[128,256]{1,0:T(8,128)(2,1)} async-done(((bf16[2048,256]{1,0:T(8,128)(2,1)}), bf16[128,256]{1,0:T(8,128)(2,1)}) %reduce-scatter.6.cloned.1.call-update) | async-done | bytes 65552
  260.8 0.9 copy.38
  261.8 0.7 copy.33
  262.5 0.7 copy.34
  263.2 4.6 %all-to-all-done = bf16[32,12,2048]{2,1,0:T(8,128)(2,1)} async-done(((bf16[32,12,2048]{2,1,0:T(8,128)(2,1)}), bf16[32,12,2048]{2,1,0:T(8,128)(2,1)}, u32[]{:S(2)}, u32[]{:S(2)}) %all-to-all-start) | async-done | bytes 1572896 | tf_op jit(solution)/shard_map/all_to_all | solution.py:45
  267.8 3.6 %reshape.13 = bf16[384,2048]{1,0:T(8,128)(2,1)} reshape(bf16[32,12,2048]{2,1,0:T(8,128)(2,1)} %all-to-all-done) | data formatting | bytes 3145728 | tf_op jit(solution)/shard_map/reshape | solution.py:44
  (4 shorter events, 0.1 us)
Async XLA Ops:
  7.2 38.0 %copy-start = (bf16[384,2048]{1,0:T(8,128)(2,1)S(1)}, bf16[384,2048]{1,0:T(8,128)(2,1)}, u32[]{:S(2)}) copy-start(bf16[384,2048]{1,0:T(8,128)(2,1)} %param.8) | copy-start | bytes 4718596
  27.3 20.8 %copy-start.3 = (bf16[2048,128]{1,0:T(8,128)(2,1)}, bf16[2048,128]{1,0:T(8,128)(2,1)S(1)}, u32[]{:S(2)}) copy-start(bf16[2048,128]{1,0:T(8,128)(2,1)S(1)} %all_gather.7) | copy-start | bytes 1572868
  45.2 2.3 copy-start.1
  45.2 1.7 copy-start.8
  122.4 24.8 %collective-permute-start.6 = (bf16[16,2048]{1,0:T(8,128)(2,1)S(1)}, bf16[16,2048]{1,0:T(8,128)(2,1)S(1)}, u32[]{:S(2)}, u32[]{:S(2)}) collective-permute-start(bf16[16,2048]{1,0:T(8,128)(2,1)S(1)} %fusion), channel_id=1, source_target_pairs={{0,7},{1,8},{2,9},{3,10},{4,11},{5,12},{6,13},{7,14},{8,15},{9,16}... | collective-permute-start | bytes 196616
  126.0 24.0 %collective-permute-start.5 = (bf16[16,2048]{1,0:T(8,128)(2,1)S(1)}, bf16[16,2048]{1,0:T(8,128)(2,1)S(1)}, u32[]{:S(2)}, u32[]{:S(2)}) collective-permute-start(bf16[16,2048]{1,0:T(8,128)(2,1)S(1)} %fusion), channel_id=1, source_target_pairs={{0,6},{1,7},{2,8},{3,9},{4,10},{5,11},{6,12},{7,13},{8,14},{9,15},... | collective-permute-start | bytes 196616
  130.3 15.3 %collective-permute-start.7 = (bf16[12,2048]{1,0:T(8,128)(2,1)S(1)}, bf16[12,2048]{1,0:T(8,128)(2,1)S(1)}, u32[]{:S(2)}, u32[]{:S(2)}) collective-permute-start(bf16[12,2048]{1,0:T(8,128)(2,1)S(1)} %slice.10), channel_id=1, source_target_pairs={{0,8},{1,9},{2,10},{3,11},{4,12},{5,13},{6,14},{7,15},{8,16},{9,17... | collective-permute-start | bytes 147464
  136.9 17.2 %collective-permute-start.4 = (bf16[16,2048]{1,0:T(8,128)(2,1)S(1)}, bf16[16,2048]{1,0:T(8,128)(2,1)S(1)}, u32[]{:S(2)}, u32[]{:S(2)}) collective-permute-start(bf16[16,2048]{1,0:T(8,128)(2,1)S(1)} %fusion), channel_id=1, source_target_pairs={{0,5},{1,6},{2,7},{3,8},{4,9},{5,10},{6,11},{7,12},{8,13},{9,14},{... | collective-permute-start | bytes 196616
  138.2 15.9 %collective-permute-start.3 = (bf16[16,2048]{1,0:T(8,128)(2,1)S(1)}, bf16[16,2048]{1,0:T(8,128)(2,1)S(1)}, u32[]{:S(2)}, u32[]{:S(2)}) collective-permute-start(bf16[16,2048]{1,0:T(8,128)(2,1)S(1)} %fusion), channel_id=1, source_target_pairs={{0,4},{1,5},{2,6},{3,7},{4,8},{5,9},{6,10},{7,11},{8,12},{9,13},{1... | collective-permute-start | bytes 196616
  145.5 8.6 %collective-permute-start.2 = (bf16[16,2048]{1,0:T(8,128)(2,1)S(1)}, bf16[16,2048]{1,0:T(8,128)(2,1)S(1)}, u32[]{:S(2)}, u32[]{:S(2)}) collective-permute-start(bf16[16,2048]{1,0:T(8,128)(2,1)S(1)} %fusion), channel_id=1, source_target_pairs={{0,3},{1,4},{2,5},{3,6},{4,7},{5,8},{6,9},{7,10},{8,11},{9,12},{10... | collective-permute-start | bytes 196616
  147.2 6.9 %collective-permute-start.1 = (bf16[16,2048]{1,0:T(8,128)(2,1)S(1)}, bf16[16,2048]{1,0:T(8,128)(2,1)S(1)}, u32[]{:S(2)}, u32[]{:S(2)}) collective-permute-start(bf16[16,2048]{1,0:T(8,128)(2,1)S(1)} %fusion), channel_id=1, source_target_pairs={{0,2},{1,3},{2,4},{3,5},{4,6},{5,7},{6,8},{7,9},{8,10},{9,11},{10,... | collective-permute-start | bytes 196616
  150.0 4.2 %collective-permute-start = (bf16[16,2048]{1,0:T(8,128)(2,1)S(1)}, bf16[16,2048]{1,0:T(8,128)(2,1)S(1)}, u32[]{:S(2)}, u32[]{:S(2)}) collective-permute-start(bf16[16,2048]{1,0:T(8,128)(2,1)S(1)} %fusion), channel_id=1, source_target_pairs={{0,1},{1,2},{2,3},{3,4},{4,5},{5,6},{6,7},{7,8},{8,9},{9,10},{10,1... | collective-permute-start | bytes 196616
  157.2 110.6 %all-to-all-start = ((bf16[32,12,2048]{2,1,0:T(8,128)(2,1)}), bf16[32,12,2048]{2,1,0:T(8,128)(2,1)}, u32[]{:S(2)}, u32[]{:S(2)}) async-start(bf16[32,12,2048]{2,1,0:T(8,128)(2,1)} %stack.2), calls=%async_computation | async-start | bytes 4194304 | tf_op jit(solution)/shard_map/all_to_all | solution.py:45
  169.5 91.3 %reduce-scatter.6.cloned.1.call-start = ((), (), s32[]{:S(2)}) async-start(), calls=%async_computation.2 | async-start | bytes 1114112
  170.2 1.4 copy-start.6
  170.3 1.5 copy-start.7
  170.3 1.6 copy-start.2
  171.6 2.4 copy-start.4
  171.8 2.1 copy-start.5
Sparse Core Ops, SparseCore 0:
  174.9 85.7 reduce-scatter.5
